TPU v7x, 32 devices: a whole 2x2x4 slice. The times are simulated.
32 devices in a mesh: sp: 4 (over z), dp: 8 (over y, x, core).
Axes of the slice: x: 2, y: 2, z: 4, core: 2. Of those that a mesh axis runs over, the one named last changes fastest.
Arguments:
- probe_vectors: bfloat16 [4096, 1024], P(('dp', 'sp')), may hold values from -6 to 6
- address_vectors: bfloat16 [4096, 1024], P(('dp', 'sp')), may hold values from -6 to 6
- content_vectors: bfloat16 [4096, 2048], P(('dp', 'sp')), may hold values from -6 to 6
- adjoint_of_result: bfloat16 [4096, 2048], P(('dp', 'sp')), may hold values from -0.5 to 0.5
- compact_factor: bfloat16 [4096, 64], P(('dp', 'sp')), may hold values from -7.5 to 7.5
- latent_to_damping_map: bfloat16 [64, 1024], replicated, may hold values from -0.75 to 0.75
- damping_shift_term: float32 [1024], replicated
- surplus_damping: bfloat16 [4096, 16], P(('dp', 'sp')), may hold values from -0.7 to 0
Outputs:
- query_grad: bfloat16 [4096, 1024], P(('dp', 'sp'))
- key_grad: bfloat16 [4096, 1024], P(('dp', 'sp'))
- value_grad: bfloat16 [4096, 2048], P(('dp', 'sp'))
- latent_grad: bfloat16 [4096, 64], P(('dp', 'sp'))
- weight_grad: float32 [64, 1024], replicated
All inputs are finite; a program needn't handle non-finite values.
Results may differ from a plain program's by a relative error of at most 0.005.
Values may be sent and summed in bfloat16 or wider, within the bound.
A program may use at most 64 MiB of HBM per device.

v0:
```python
import jax
import jax.numpy as jnp
from jax import lax
from jax.sharding import PartitionSpec as P

KEY_CHANNELS = 64
VALUE_DIM = 128
BLOCK = 64


gate_norm = 16.0
highest = lax.Precision.HIGHEST


def carry_states(block_total, increments):
    log_totals = block_total[:, :, 0, :]
    running = jnp.cumsum(log_totals, axis=1)
    before = running - log_totals
    blocks = log_totals.shape[1]
    order = jnp.arange(blocks, dtype=jnp.int32)
    earlier_mask = (order[None, :] < order[:, None])[None, :, :, None]
    exponent = before[:, :, None, :] - running[:, None, :, :]
    exponent = jnp.where(earlier_mask, exponent, jnp.zeros_like(exponent))
    weights = jnp.where(earlier_mask, jnp.exp(exponent), jnp.zeros_like(exponent))
    return jnp.einsum("hnmk,mhkv->nhkv", weights, increments, precision=highest)


def gla_forward(probe_vectors, address_vectors, content_vectors, logarithm_decay):
    head_count, seq_len, key_width = probe_vectors.shape
    value_width = content_vectors.shape[2]
    blocks = seq_len // BLOCK

    def blocked(tensor):
        return tensor.reshape(head_count, blocks, BLOCK, tensor.shape[2])

    cumulative = jnp.cumsum(blocked(logarithm_decay), axis=2)
    block_total = cumulative[:, :, BLOCK - 1 :, :]
    keys_block = blocked(address_vectors)
    query_decayed = blocked(probe_vectors) * key_width ** (-0.5) * jnp.exp(cumulative)
    key_inverse = keys_block * jnp.exp(-cumulative)
    key_to_end = keys_block * jnp.exp(block_total - cumulative)
    value_block = blocked(content_vectors)
    scores = jnp.einsum("hnik,hnjk->hnij", query_decayed, key_inverse, precision=highest)
    positions = jnp.arange(BLOCK, dtype=jnp.int32)
    causal = positions[:, None] >= positions[None, :]
    scores = jnp.where(causal, scores, jnp.zeros_like(scores))
    within_block = jnp.einsum("hnij,hnjv->hniv", scores, value_block, precision=highest)
    increments = jnp.einsum("hnjk,hnjv->nhkv", key_to_end, value_block, precision=highest)
    earlier = carry_states(block_total, increments)
    carried = jnp.einsum("hnik,nhkv->hniv", query_decayed, earlier, precision=highest)
    return (within_block + carried).reshape(head_count, seq_len, value_width)


def split_into_heads(tensor, width):
    return tensor.astype(jnp.float32).reshape(tensor.shape[0], -1, width).transpose(1, 0, 2)


def to_rows(tensor):
    return tensor.transpose(1, 0, 2).reshape(tensor.shape[1], tensor.shape[0] * tensor.shape[2])


def on_device(
    probe_vectors,
    address_vectors,
    content_vectors,
    adjoint_of_result,
    compact_factor,
    latent_to_damping_map,
    damping_shift_term,
    surplus_damping,
):
    query_per_head, key_per_head, value_per_head, upstream_heads, spike_heads = (
        lax.all_to_all(probe_vectors, "sp", split_axis=1, concat_axis=0, tiled=True),
        lax.all_to_all(address_vectors, "sp", split_axis=1, concat_axis=0, tiled=True),
        lax.all_to_all(content_vectors, "sp", split_axis=1, concat_axis=0, tiled=True),
        lax.all_to_all(adjoint_of_result, "sp", split_axis=1, concat_axis=0, tiled=True),
        lax.all_to_all(surplus_damping, "sp", split_axis=1, concat_axis=0, tiled=True),
    )
    local_width = query_per_head.shape[1]
    hidden_code_rows = lax.all_gather(compact_factor, "sp", axis=0, tiled=True)
    column_start = lax.axis_index("sp") * local_width
    weight_local = lax.dynamic_slice_in_dim(latent_to_damping_map, column_start, local_width, 1)
    bias_local = lax.dynamic_slice_in_dim(damping_shift_term, column_start, local_width, 0)
    gate_logit = (
        jnp.dot(hidden_code_rows, weight_local, preferred_element_type=jnp.float32) + bias_local
    )
    forget_rate_rows = jax.nn.log_sigmoid(gate_logit) / gate_norm
    logarithm_decay = (
        split_into_heads(forget_rate_rows, KEY_CHANNELS)
        + spike_heads.astype(jnp.float32).T[:, :, None]
    )
    _, pullback = jax.vjp(
        gla_forward,
        split_into_heads(query_per_head, KEY_CHANNELS),
        split_into_heads(key_per_head, KEY_CHANNELS),
        split_into_heads(value_per_head, VALUE_DIM),
        logarithm_decay,
    )
    grad_query, grad_key, grad_value, grad_decay = pullback(
        split_into_heads(upstream_heads, VALUE_DIM)
    )
    query_grad, key_grad, value_grad = (
        lax.all_to_all(
            to_rows(grad_query).astype(jnp.bfloat16), "sp", split_axis=0, concat_axis=1, tiled=True
        ),
        lax.all_to_all(
            to_rows(grad_key).astype(jnp.bfloat16), "sp", split_axis=0, concat_axis=1, tiled=True
        ),
        lax.all_to_all(
            to_rows(grad_value).astype(jnp.bfloat16), "sp", split_axis=0, concat_axis=1, tiled=True
        ),
    )
    decay_rows = to_rows(grad_decay)
    gate_grad = (decay_rows * jax.nn.sigmoid(-gate_logit) / gate_norm).astype(jnp.bfloat16)
    partial_latent = jnp.einsum(
        "sc,rc->sr", gate_grad, weight_local, preferred_element_type=jnp.float32
    )
    latent_grad = lax.psum_scatter(partial_latent, "sp", scatter_dimension=0, tiled=True).astype(
        jnp.bfloat16
    )
    local_weight = jnp.einsum(
        "sr,sc->rc", hidden_code_rows, gate_grad, preferred_element_type=jnp.float32
    )
    summed = lax.psum(local_weight, "dp")
    weight_grad = lax.all_gather(summed, "sp", axis=1, tiled=True)
    return (query_grad, key_grad, value_grad, latent_grad, weight_grad)


def solution(mesh):
    return jax.shard_map(
        on_device,
        mesh=mesh,
        in_specs=(
            P(("dp", "sp"), None),
            P(("dp", "sp"), None),
            P(("dp", "sp"), None),
            P(("dp", "sp"), None),
            P(("dp", "sp"), None),
            P(),
            P(),
            P(("dp", "sp"), None),
        ),
        out_specs=(
            P(("dp", "sp"), None),
            P(("dp", "sp"), None),
            P(("dp", "sp"), None),
            P(("dp", "sp"), None),
            P(),
        ),
        check_vma=False,
    )
```

profile of v0, /device:TPU:0, one launch (start us, length us, event | category | flops | bytes accessed | tf_op | source)
XLA Modules:
  0.0 277.0 jit_solution(3052615414394250195)
XLA Ops:
  8.0 6.5 %all-to-all-start.1 = ((bf16[128,4,4]{0,2,1:T(4,128)(2,1)}), bf16[128,4,4]{0,2,1:T(4,128)(2,1)S(1)}, u32[]{:S(2)}, u32[]{:S(2)}) async-start(bf16[128,4,4]{0,2,1:T(4,128)(2,1)} %bitcast.169), calls=%async_computation.1 | async-start | bytes 8192 | tf_op jit(solution)/shard_map/all_to_all | solution.py:77
  14.5 1.8 copy.214
  16.3 3.8 %all-to-all-done.1 = bf16[128,4,4]{0,2,1:T(4,128)(2,1)S(1)} async-done(((bf16[128,4,4]{0,2,1:T(4,128)(2,1)}), bf16[128,4,4]{0,2,1:T(4,128)(2,1)S(1)}, u32[]{:S(2)}, u32[]{:S(2)}) %all-to-all-start.1) | async-done | bytes 4128 | tf_op jit(solution)/shard_map/all_to_all | solution.py:77
  20.1 3.5 %all-to-all-start.5 = ((bf16[128,4,256]{0,2,1:T(8,128)(2,1)}), bf16[128,4,256]{0,2,1:T(8,128)(2,1)S(1)}, u32[]{:S(2)}, u32[]{:S(2)}) async-start(bf16[128,4,256]{0,2,1:T(8,128)(2,1)} %bitcast.24), calls=%async_computation.5 | async-start | bytes 524288 | tf_op jit(solution)/shard_map/all_to_all | solution.py:73
  24.5 7.0 %all-to-all-done.5 = bf16[128,4,256]{0,2,1:T(8,128)(2,1)S(1)} async-done(((bf16[128,4,256]{0,2,1:T(8,128)(2,1)}), bf16[128,4,256]{0,2,1:T(8,128)(2,1)S(1)}, u32[]{:S(2)}, u32[]{:S(2)}) %all-to-all-start.5) | async-done | bytes 262176 | tf_op jit(solution)/shard_map/all_to_all | solution.py:73
  31.5 3.4 %all-to-all-start = ((bf16[128,4,256]{0,2,1:T(8,128)(2,1)}), bf16[128,4,256]{0,2,1:T(8,128)(2,1)S(1)}, u32[]{:S(2)}, u32[]{:S(2)}) async-start(bf16[128,4,256]{0,2,1:T(8,128)(2,1)} %bitcast), calls=%async_computation | async-start | bytes 524288 | tf_op jit(solution)/shard_map/all_to_all | solution.py:74
  36.6 12.5 %all_gather.6 = bf16[512,64]{0,1:T(8,128)(2,1)S(1)} all-gather(bf16[128,64]{0,1:T(8,128)(2,1)S(1)} %copy-done.31), channel_id=1, replica_groups=mesh['sp'=4,'dp'=8] {'sp'}, dimensions={0}, use_global_device_ids=true | all-gather | bytes 81920 | tf_op jit(solution)/shard_map/all_gather | solution.py:80
  49.7 1.3 fusion.20
  51.7 4.1 %all-to-all-start.3 = ((bf16[128,4,512]{2,0,1:T(8,128)(2,1)}), bf16[128,4,512]{2,0,1:T(8,128)(2,1)}, u32[]{:S(2)}, u32[]{:S(2)}) async-start(bf16[128,4,512]{2,0,1:T(8,128)(2,1)} %bitcast.143), calls=%async_computation.3 | async-start | bytes 1048576 | tf_op jit(solution)/shard_map/all_to_all | solution.py:76
  56.4 0.9 copy.312
  58.0 25.9 %fusion.46 = f32[4,8,64,64]{3,1,2,0:T(8,128)S(1)} fusion(f32[4,8,64,64]{3,1,2,0:T(8,128)S(1)} %copy.194), kind=kOutput, calls=%fused_computation.84 | output fusion | flops 8257536 | bytes 1048576 | tf_op jit(solution)/shard_map/jvp(jit(cumsum))/reduce_window_sum | solution.py:36
  83.9 5.1 %all-to-all-start.2 = ((bf16[128,4,512]{2,0,1:T(8,128)(2,1)}), bf16[128,4,512]{2,0,1:T(8,128)(2,1)}, u32[]{:S(2)}, u32[]{:S(2)}) async-start(bf16[128,4,512]{2,0,1:T(8,128)(2,1)} %bitcast.144), calls=%async_computation.2 | async-start | bytes 1048576 | tf_op jit(solution)/shard_map/all_to_all | solution.py:75
  92.8 1.0 reshape.170
  93.8 1.2 reshape.166
  95.1 2.0 reshape.161
  97.0 1.9 copy.205
  99.4 2.0 reshape.159
  101.3 1.2 copy.198
  102.6 0.9 convolution_bitcast_fusion.3
  103.7 2.9 %convolution_bitcast_fusion = f32[8,4,64,128]{3,0,2,1:T(8,128)S(1)} fusion(f32[4,64,128,8]{2,1,3,0:T(8,128)S(1)} %convolution_bitcast_fusion.3, f32[4,8,64]{1,2,0:T(8,128)S(1)} %copy-done.23, f32[4,8,64]{1,2,0:T(8,128)S(1)} %copy-done.24, pred[8,8]{1,0:T(8,128)(4,1)S(1)} %copy-done.32), kind=kOutput, calls=%fused_computation.4 | convolution fusion | flops 25214976 | bytes 2113600 | tf_op jit(solution)/shard_map/transpose(jvp(hnmk,mhkv->nhkv))/dot_general | solution.py:25
  106.6 2.8 %fusion.18 = (f32[4,8,64]{2,1,0:T(8,128)}, f32[4,8,64,64]{2,3,1,0:T(8,128)S(1)}, f32[4,8,64,64]{2,3,1,0:T(8,128)}) fusion(f32[4,8,64,64]{2,3,1,0:T(8,128)S(1)} %copy.195, f32[4,8,64,64]{2,1,3,0:T(8,128)S(1)} %reshape.166, f32[4,8,64]{2,1,0:T(8,128)S(1)} %slice_bitcast_fusion, bf16[4,8,64,128]{3,2,1,0:T(8,128)(2,1)S(1)} %bitcast.150, ...), kind=kOutput, calls=%fused_computation.40 | convolution fusion | flops 201979904 | bytes 3686400 | tf_op jit(solution)/shard_map/transpose(jvp(hnjk,hnjv->nhkv))/dot_general | solution.py:48
  110.4 2.5 convolution_bitcast_fusion.1
  112.9 4.3 %fusion.45 = (f32[4,8,64]{1,2,0:T(8,128)}, f32[4,8,64]{1,2,0:T(8,128)}) fusion(f32[4,8,64]{1,2,0:T(8,128)S(1)} %copy-done.23, f32[4,8,64]{1,2,0:T(8,128)S(1)} %copy-done.24, f32[8,4,64,128]{3,2,1,0:T(8,128)S(1)} %fusion.6, f32[4,64,128,8]{2,1,3,0:T(8,128)S(1)} %convolution_bitcast_fusion.3, pred[8,8]{1,0:T(8,128)(4,1)S(1)} %copy-done.32), kind=kOutput, calls=%fused_computation.83 | convolution fusion | flops 25276416 | bytes 2129984 | tf_op jit(solution)/shard_map/transpose(jvp(hnmk,mhkv->nhkv))/dot_general | solution.py:25
  117.3 2.0 convolution_bitcast_fusion.4
  120.9 1.4 copy.243
  122.2 1.4 copy.244
  123.6 1.4 copy.245
  125.1 1.6 convolution_select_fusion
  126.7 1.3 fusion.44
  128.6 1.5 fusion.3
  130.1 3.7 %pad_add_fusion = (f32[4,8,64,64]{2,3,1,0:T(8,128)}, bf16[4,8,64,64]{2,3,1,0:T(8,128)(2,1)}, bf16[4,8,64,64]{2,3,1,0:T(8,128)(2,1)S(1)}) fusion(f32[4,8,1,64]{2,3,1,0:T(8,128)S(1)} %fusion.3, f32[4,8,64,64]{2,3,1,0:T(8,128)S(1)} %fusion.44, f32[4,8,64,64]{2,1,3,0:T(8,128)S(1)} %mul.72, f32[4,8,64,64]{2,3,1,0:T(8,128)S(1)} %copy.195, ...), kind=kOutput, calls=%fused_computation.22 | convolution fusion | flops 103677952 | bytes 4734976 | tf_op jit(solution)/shard_map/transpose(jvp(hnik,hnjk->hnij))/dot_general | solution.py:43
  133.8 1.1 copy.212
  134.9 1.4 convert_element_type.73
  137.1 1.7 copy.213
  138.8 4.8 %all-to-all-start.4 = ((bf16[4,128,256]{1,2,0:T(8,128)(2,1)}), bf16[4,128,256]{1,2,0:T(8,128)(2,1)S(1)}, u32[]{:S(2)}, u32[]{:S(2)}) async-start(bf16[4,128,256]{1,2,0:T(8,128)(2,1)} %copy.213), calls=%async_computation.4 | async-start | bytes 524288 | tf_op jit(solution)/shard_map/all_to_all | solution.py:103
  143.6 3.1 %convolution_select_fusion.2 = f32[4,8,64,64]{3,2,1,0:T(8,128)} fusion(pred[64,64]{1,0:T(8,128)(4,1)S(1)} %copy-done.28, f32[4,8,64,64]{2,1,3,0:T(8,128)S(1)} %reshape.166, f32[4,8,64,64]{2,3,1,0:T(8,128)S(1)} %copy.195, f32[4,8,64,64]{2,1,3,0:T(8,128)S(1)} %mul.72), kind=kOutput, calls=%fused_computation.11 | convolution fusion | flops 101187584 | bytes 2101248 | tf_op jit(solution)/shard_map/jvp(hnik,hnjk->hnij)/dot_general | solution.py:43
  148.3 3.2 %fusion.11 = f32[4,8,64,128]{3,2,1,0:T(8,128)S(1)} fusion(f32[4,8,64,64]{2,3,1,0:T(8,128)S(1)} %copy-done.4, f32[8,4,64,128]{3,0,2,1:T(8,128)} %copy-done.9), kind=kOutput, calls=%fused_computation.30 | convolution fusion | flops 201326592 | bytes 2621440 | tf_op jit(solution)/shard_map/transpose(jvp(hnjk,hnjv->nhkv))/dot_general | solution.py:48
  151.5 5.2 %all-to-all-start.6 = ((bf16[4,128,256]{1,2,0:T(8,128)(2,1)}), bf16[4,128,256]{1,2,0:T(8,128)(2,1)S(1)}, u32[]{:S(2)}, u32[]{:S(2)}) async-start(bf16[4,128,256]{1,2,0:T(8,128)(2,1)} %copy.226), calls=%async_computation.6 | async-start | bytes 524288 | tf_op jit(solution)/shard_map/all_to_all | solution.py:106
  156.7 1.0 fusion.4
  158.2 1.0 convert_element_type.84
  159.6 25.8 %fusion.47 = f32[4,8,64,64]{3,1,2,0:T(8,128)S(1)} fusion(f32[4,8,64,64]{3,1,2,0:T(8,128)S(1)} %copy.246), kind=kOutput, calls=%fused_computation.85 | output fusion | flops 8257536 | bytes 1048576 | tf_op jit(solution)/shard_map/transpose(jvp(jit(cumsum)))/reduce_window_sum | solution.py:36
  186.1 5.2 %all-to-all-start.7 = ((bf16[4,128,512]{2,1,0:T(8,128)(2,1)}), bf16[4,128,512]{2,1,0:T(8,128)(2,1)S(1)}, u32[]{:S(2)}, u32[]{:S(2)}) async-start(bf16[4,128,512]{2,1,0:T(8,128)(2,1)} %convert_element_type.84), calls=%async_computation.7 | async-start | bytes 1048576 | tf_op jit(solution)/shard_map/all_to_all | solution.py:109
  193.9 56.5 %all-reduce.3.cloned.1.call-done = f32[64,256]{1,0:T(8,128)} async-done(((f32[64,256]{1,0:T(8,128)}), f32[64,256]{1,0:T(8,128)}) %all-reduce.3.cloned.1.call-update) | async-done | bytes 65552 | tf_op jit(solution)/shard_map/psum | solution.py:124
  250.4 14.1 %all_gather.7 = f32[64,1024]{1,0:T(8,128)S(1)} all-gather(f32[64,256]{1,0:T(8,128)} %all-reduce.3.cloned.1.call-done), channel_id=1, replica_groups=mesh['sp'=4,'dp'=8] {'sp'}, dimensions={1}, use_global_device_ids=true | all-gather | bytes 327680 | tf_op jit(solution)/shard_map/all_gather | solution.py:125
  264.5 1.4 convert_element_type.86
  265.9 0.8 copy.248
  266.7 0.8 copy.249
  267.9 1.0 copy.250
  (116 shorter events, 20.1 us)
Async XLA Ops:
  8.0 41.7 %copy-start = (bf16[64,1024]{1,0:T(8,128)(2,1)S(1)}, bf16[64,1024]{1,0:T(8,128)(2,1)}, u32[]{:S(2)}) copy-start(bf16[64,1024]{1,0:T(8,128)(2,1)} %param.13) | copy-start | bytes 393220
  8.0 12.1 %all-to-all-start.1 = ((bf16[128,4,4]{0,2,1:T(4,128)(2,1)}), bf16[128,4,4]{0,2,1:T(4,128)(2,1)S(1)}, u32[]{:S(2)}, u32[]{:S(2)}) async-start(bf16[128,4,4]{0,2,1:T(4,128)(2,1)} %bitcast.169), calls=%async_computation.1 | async-start | bytes 8192 | tf_op jit(solution)/shard_map/all_to_all | solution.py:77
  20.1 3.6 %copy-start.20 = (bf16[128,1024]{1,0:T(8,128)(2,1)S(1)}, bf16[128,1024]{1,0:T(8,128)(2,1)}, u32[]{:S(2)}) copy-start(bf16[128,1024]{1,0:T(8,128)(2,1)} %param.9) | copy-start | bytes 786436
  20.1 11.4 %all-to-all-start.5 = ((bf16[128,4,256]{0,2,1:T(8,128)(2,1)}), bf16[128,4,256]{0,2,1:T(8,128)(2,1)S(1)}, u32[]{:S(2)}, u32[]{:S(2)}) async-start(bf16[128,4,256]{0,2,1:T(8,128)(2,1)} %bitcast.24), calls=%async_computation.5 | async-start | bytes 524288 | tf_op jit(solution)/shard_map/all_to_all | solution.py:73
  23.6 11.3 %copy-start.17 = (bf16[128,2048]{1,0:T(8,128)(2,1)S(1)}, bf16[128,2048]{1,0:T(8,128)(2,1)}, u32[]{:S(2)}) copy-start(bf16[128,2048]{1,0:T(8,128)(2,1)} %param.11) | copy-start | bytes 1572868
  31.5 19.5 %all-to-all-start = ((bf16[128,4,256]{0,2,1:T(8,128)(2,1)}), bf16[128,4,256]{0,2,1:T(8,128)(2,1)S(1)}, u32[]{:S(2)}, u32[]{:S(2)}) async-start(bf16[128,4,256]{0,2,1:T(8,128)(2,1)} %bitcast), calls=%async_computation | async-start | bytes 524288 | tf_op jit(solution)/shard_map/all_to_all | solution.py:74
  35.0 1.6 copy-start.31
  49.0 1.9 copy-start.21
  51.0 0.7 copy-start.15
  51.0 5.4 %copy-start.18 = (bf16[128,2048]{1,0:T(8,128)(2,1)S(1)}, bf16[128,2048]{1,0:T(8,128)(2,1)}, u32[]{:S(2)}) copy-start(bf16[128,2048]{1,0:T(8,128)(2,1)} %param.10) | copy-start | bytes 1572868
  51.7 32.2 %all-to-all-start.3 = ((bf16[128,4,512]{2,0,1:T(8,128)(2,1)}), bf16[128,4,512]{2,0,1:T(8,128)(2,1)}, u32[]{:S(2)}, u32[]{:S(2)}) async-start(bf16[128,4,512]{2,0,1:T(8,128)(2,1)} %bitcast.143), calls=%async_computation.3 | async-start | bytes 1048576 | tf_op jit(solution)/shard_map/all_to_all | solution.py:76
  83.9 15.5 %all-to-all-start.2 = ((bf16[128,4,512]{2,0,1:T(8,128)(2,1)}), bf16[128,4,512]{2,0,1:T(8,128)(2,1)}, u32[]{:S(2)}, u32[]{:S(2)}) async-start(bf16[128,4,512]{2,0,1:T(8,128)(2,1)} %bitcast.144), calls=%async_computation.2 | async-start | bytes 1048576 | tf_op jit(solution)/shard_map/all_to_all | solution.py:75
  91.5 1.0 copy-start.16
  101.3 1.2 copy-start.1
  102.5 7.0 %copy-start.5 = (bf16[4,512,128]{2,1,0:T(8,128)(2,1)}, bf16[4,512,128]{2,1,0:T(8,128)(2,1)S(1)}, u32[]{:S(2)}) copy-start(bf16[4,512,128]{2,1,0:T(8,128)(2,1)S(1)} %copy.198) | copy-start | bytes 1572868
  102.5 1.1 copy-start.23
  102.5 1.1 copy-start.24
  102.5 1.1 copy-start.32
  106.6 2.9 %copy-start.9 = (f32[8,4,64,128]{3,0,2,1:T(8,128)}, f32[8,4,64,128]{3,0,2,1:T(8,128)S(1)}, u32[]{:S(2)}) copy-start(f32[8,4,64,128]{3,0,2,1:T(8,128)S(1)} %convolution_bitcast_fusion) | copy-start | bytes 3145732
  109.5 1.0 copy-start.3
  117.3 2.0 copy-start.26
  119.2 0.9 copy-start.25
  120.1 0.7 copy-start.30
  122.2 1.4 copy-start.29
  123.6 1.4 copy-start.27
  126.7 1.3 copy-start.11
  126.7 1.5 copy-start.12
  126.7 1.8 copy-start.13
  128.5 1.5 copy-start.8
  128.5 1.5 copy-start.10
  138.8 4.8 %copy-start.28 = (pred[64,64]{1,0:T(8,128)(4,1)S(1)}, pred[64,64]{1,0:T(8,128)(4,1)}, u32[]{:S(2)}) copy-start(pred[64,64]{1,0:T(8,128)(4,1)} %iota_compare_fusion) | copy-start | bytes 12292
  138.8 12.7 %all-to-all-start.4 = ((bf16[4,128,256]{1,2,0:T(8,128)(2,1)}), bf16[4,128,256]{1,2,0:T(8,128)(2,1)S(1)}, u32[]{:S(2)}, u32[]{:S(2)}) async-start(bf16[4,128,256]{1,2,0:T(8,128)(2,1)} %copy.213), calls=%async_computation.4 | async-start | bytes 524288 | tf_op jit(solution)/shard_map/all_to_all | solution.py:103
  143.6 3.1 %copy-start.14 = (bf16[4,8,64,64]{2,3,1,0:T(8,128)(2,1)S(1)}, bf16[4,8,64,64]{2,3,1,0:T(8,128)(2,1)}, u32[]{:S(2)}) copy-start(bf16[4,8,64,64]{2,3,1,0:T(8,128)(2,1)} %get-tuple-element.23) | copy-start | bytes 786436
  147.1 1.2 copy-start.4
  148.3 8.4 %copy-start.6 = (f32[4,8,64,64]{3,2,1,0:T(8,128)S(1)}, f32[4,8,64,64]{3,2,1,0:T(8,128)}, u32[]{:S(2)}) copy-start(f32[4,8,64,64]{3,2,1,0:T(8,128)} %convolution_select_fusion.2) | copy-start | bytes 1572868
  151.5 5.3 %copy-start.2 = (bf16[4,512,128]{2,1,0:T(8,128)(2,1)S(1)}, bf16[4,512,128]{2,1,0:T(8,128)(2,1)}, u32[]{:S(2)}) copy-start(bf16[4,512,128]{2,1,0:T(8,128)(2,1)} %copy.205) | copy-start | bytes 1572868
  151.5 34.6 %all-to-all-start.6 = ((bf16[4,128,256]{1,2,0:T(8,128)(2,1)}), bf16[4,128,256]{1,2,0:T(8,128)(2,1)S(1)}, u32[]{:S(2)}, u32[]{:S(2)}) async-start(bf16[4,128,256]{1,2,0:T(8,128)(2,1)} %copy.226), calls=%async_computation.6 | async-start | bytes 524288 | tf_op jit(solution)/shard_map/all_to_all | solution.py:106
  157.7 1.4 copy-start.7
  186.1 5.3 %copy-start.19 = (f32[256,512]{1,0:T(8,128)S(1)}, f32[256,512]{1,0:T(8,128)}, u32[]{:S(2)}) copy-start(f32[256,512]{1,0:T(8,128)} %get-tuple-element.30) | copy-start | bytes 1572868
  186.1 81.5 %all-to-all-start.7 = ((bf16[4,128,512]{2,1,0:T(8,128)(2,1)}), bf16[4,128,512]{2,1,0:T(8,128)(2,1)S(1)}, u32[]{:S(2)}, u32[]{:S(2)}) async-start(bf16[4,128,512]{2,1,0:T(8,128)(2,1)} %convert_element_type.84), calls=%async_computation.7 | async-start | bytes 1048576 | tf_op jit(solution)/shard_map/all_to_all | solution.py:109
  191.3 59.1 %all-reduce.3.cloned.1.call-start = ((), (), s32[]{:S(2)}) async-start(), calls=%async_computation.10 | async-start | bytes 131072 | tf_op jit(solution)/shard_map/psum | solution.py:124
  191.3 0.8 copy-start.22
  193.0 71.5 %reduce-scatter.2.cloned.1.call-start = ((), (), s32[]{:S(2)}) async-start(), calls=%async_computation.9 | async-start | bytes 163840 | tf_op jit(solution)/shard_map/reduce_scatter | solution.py:118
Sparse Core Ops, SparseCore 0:
  195.7 54.6 all-reduce.2
Sparse Core Ops, SparseCore 1:
  196.3 20.9 reduce-scatter.1
where the time goes:
time: 279 us; the launch traced here: 277 us
  waiting for transfers between devices  67.7 us (24%)
  other arithmetic  56 us (20%)
  local copies, waits for them, and re-layouts  39.8 us (14%)
  starting transfers between devices  38 us (14%)
  matrix products  32.9 us (12%)
  blocking collectives  26.6 us (10%)
  between operations  15.9 us (6%)
    psum x1, waiting for transfers between devices, on_device(): summed = lax.psum(local_weight, 'dp')  56.5 us
    another operation x2, other arithmetic, gla_forward(): cumulative = jnp.cumsum(blocked(logarithm_decay), axis=2)  51.6 us
    all_gather x1, blocking collectives, on_device(): weight_grad = lax.all_gather(summed, 'sp', axis=1, tiled=True)  14.1 us
    all_gather x1, blocking collectives, on_device(): hidden_code_rows = lax.all_gather(compact_factor, 'sp', axis=0, tiled=True)  12.5 us
    unnamed x72, local copies, waits for them, and re-layouts  10.3 us
    dot_general x3, matrix products, carry_states(): return jnp.einsum('hnmk,mhkv->nhkv', weights, increments, precision=highest)  9.75 us
    dot_general x3, matrix products, gla_forward(): jnp.einsum('hnik,hnjk->hnij', query_decayed, key_inverse, precision=highest)  8.12 us
    all_to_all x1, waiting for transfers between devices, on_device(): lax.all_to_all(probe_vectors, 'sp', split_axis=1, concat_axis=0, tiled=True)  7.02 us
  transfers between devices with their start and end apart: 10, of which 4 were waited for; matrix products, arithmetic and copies ran while one was open for 31% of the time, Pallas kernels for 0%

commit v1 on v0

v1 whole, which is shorter than its diff:
```python
import functools

import jax
import jax.numpy as jnp
from jax import lax
from jax.experimental import pallas as pl
from jax.experimental.pallas import tpu as pltpu
from jax.sharding import PartitionSpec as P

GATE_NORM = 16.0
BF = jnp.bfloat16
F32 = jnp.float32
LANES = 128


def nn(a, b):
    return lax.dot_general(a, b, (((1,), (0,)), ((), ())), preferred_element_type=F32)


def nt(a, b):
    return lax.dot_general(a, b, (((1,), (1,)), ((), ())), preferred_element_type=F32)


def tn(a, b):
    return lax.dot_general(a, b, (((0,), (0,)), ((), ())), preferred_element_type=F32)


def thirds(x, axis):
    top = x.astype(BF)
    rest = x - top.astype(F32)
    middle = rest.astype(BF)
    low = (rest - middle.astype(F32)).astype(BF)
    return jnp.concatenate([top, middle, low], axis=axis)


def kernel(
    n_sp, n_dp,
    q_ref, k_ref, v_ref, do_ref, lat_ref, map_ref, bias_ref, extra_ref,
    dq_ref, dk_ref, dv_ref, lg_ref, wg_ref,
    qd, kd, qs, ke, es, ee, gate, dec, inc, adj, dqi, dki, dvi, rin,
    s_in, s_out, g_in, g_out,
    w_own, a_src, a_dst, b_all, c_all,
    s_send, s_recv, g_send, g_recv, a_send, a_recv, b_send, b_recv, c_send, c_recv,
):
    tokens, width = q_ref.shape
    heads = extra_ref.shape[1]
    key_width = width // heads
    pairs = width // LANES
    value_width = v_ref.shape[1] // pairs
    vd = value_width // 2
    scale = key_width ** (-0.5)
    middle = tokens // 2
    rows = map_ref.shape[0] // n_sp
    me = lax.axis_index("sp")
    mine = lax.axis_index("dp")
    first = me == 0
    last = me == n_sp - 1

    barrier = pltpu.get_barrier_semaphore()
    for o in range(1, n_sp):
        pl.semaphore_signal(barrier, inc=1, device_id={"sp": lax.rem(me + o, n_sp)})
    for o in range(1, n_dp):
        pl.semaphore_signal(barrier, inc=1, device_id={"dp": lax.rem(mine + o, n_dp)})

    row = lax.broadcasted_iota(jnp.int32, (tokens, tokens), 0)
    col = lax.broadcasted_iota(jnp.int32, (tokens, tokens), 1)
    plus = (row >= middle) & (col >= middle) & (col <= row)
    minus = (row < middle) & (col < middle) & (col > row)
    prefix = (plus.astype(F32) - minus.astype(F32)).astype(BF)
    prefix = jnp.concatenate([prefix] * 3, axis=1)
    suffix = (col >= row).astype(F32).astype(BF)
    suffix = jnp.concatenate([suffix] * 3, axis=1)
    causal = jnp.concatenate([col <= row] * 2, axis=1)
    anti = jnp.concatenate([col >= row] * 2, axis=1)
    low_lane = lax.broadcasted_iota(jnp.int32, (tokens, LANES), 1) < key_width
    low_state = lax.broadcasted_iota(jnp.int32, (vd, LANES), 1) < key_width

    def stack(x, low):
        zero = jnp.zeros_like(x)
        return jnp.concatenate([jnp.where(low, x, zero), jnp.where(low, zero, x)], axis=0)

    def lanes(c):
        return slice(c * LANES, (c + 1) * LANES)

    def values(c):
        return slice(c * value_width, (c + 1) * value_width)

    def s_copy(c):
        return pltpu.make_async_remote_copy(
            src_ref=s_out.at[c], dst_ref=s_in.at[c], send_sem=s_send.at[c], recv_sem=s_recv.at[c],
            device_id={"sp": lax.rem(me + 1, n_sp)})

    def g_copy(c):
        return pltpu.make_async_remote_copy(
            src_ref=g_out.at[c], dst_ref=g_in.at[c], send_sem=g_send.at[c], recv_sem=g_recv.at[c],
            device_id={"sp": lax.rem(me + n_sp - 1, n_sp)})

    latent = lat_ref[...]
    extra = extra_ref[...]
    pl.semaphore_wait(barrier, n_sp + n_dp - 2)

    @pl.when(first)
    def _():
        s_in[...] = jnp.zeros_like(s_in)

    @pl.when(last)
    def _():
        g_in[...] = jnp.zeros_like(g_in)

    for c in range(pairs):
        at = lanes(c)
        logit = nn(latent, map_ref[:, at]) + bias_ref[:, at]
        e = jnp.exp(-jnp.abs(logit))
        gate[:, at] = jnp.where(logit >= 0, e, 1.0) / (1.0 + e) / GATE_NORM
        head_of = lax.broadcasted_iota(jnp.int32, (heads, LANES), 1) // key_width + c * (LANES // key_width)
        spread = (lax.broadcasted_iota(jnp.int32, (heads, LANES), 0) == head_of).astype(F32).astype(BF)
        log_decay = (jnp.minimum(logit, 0.0) - jnp.log1p(e)) / GATE_NORM + nn(extra, spread)
        cum = nn(prefix, thirds(log_decay, 0))
        head_total = jnp.sum(log_decay[:middle], axis=0, keepdims=True)
        end = cum[tokens - 1 :]
        dec[:, at] = jnp.exp(head_total + end)
        q = q_ref[:, at].astype(F32) * scale
        k = k_ref[:, at].astype(F32)
        e_start = jnp.exp(cum + head_total)
        e_end = jnp.exp(end - cum)
        es[:, at] = e_start * scale
        ee[:, at] = e_end
        q_start = (q * e_start).astype(BF)
        k_end = (k * e_end).astype(BF)
        qs[:, at] = q_start
        ke[:, at] = k_end
        up = jnp.exp(cum)
        down = jnp.exp(-cum)
        dqi[:, at] = up * scale
        dki[:, at] = down
        qd[:, at] = (q * up).astype(BF)
        kd[:, at] = (k * down).astype(BF)
        both = tn(v_ref[:, values(c)], k_end)
        increment = jnp.where(low_state, both[:vd], both[vd:])
        both = tn(do_ref[:, values(c)], q_start)
        adjoint = jnp.where(low_state, both[:vd], both[vd:])
        inc[c] = increment
        adj[c] = adjoint

        @pl.when(first)
        def _():
            s_out[c] = increment.astype(BF)
            s_copy(c).start()

        @pl.when(last)
        def _():
            g_out[c] = adjoint.astype(BF)
            g_copy(c).start()

    inner = jnp.logical_and(jnp.logical_not(first), jnp.logical_not(last))
    for c in range(pairs):
        at = lanes(c)

        @pl.when(jnp.logical_not(first))
        def _():
            s_copy(c).wait_recv()

        @pl.when(inner)
        def _():
            s_out[c] = (dec[:, at] * s_in[c].astype(F32) + inc[c]).astype(BF)
            s_copy(c).start()

        @pl.when(jnp.logical_not(last))
        def _():
            g_copy(c).wait_recv()

        @pl.when(inner)
        def _():
            g_out[c] = (dec[:, at] * g_in[c].astype(F32) + adj[c]).astype(BF)
            g_copy(c).start()

        qc = qd[:, at]
        kc = kd[:, at]
        q_stack = stack(qc, low_lane)
        k_stack = stack(kc, low_lane)
        v0 = v_ref[:, c * value_width : c * value_width + vd]
        v1 = v_ref[:, c * value_width + vd : (c + 1) * value_width]
        d0 = do_ref[:, c * value_width : c * value_width + vd]
        d1 = do_ref[:, c * value_width + vd : (c + 1) * value_width]
        score_t = jnp.where(anti, nt(kc, q_stack), 0.0).astype(BF)
        a = jnp.where(causal, jnp.concatenate([nt(d0, v0), nt(d1, v1)], axis=1), 0.0).astype(BF)
        a_t = jnp.where(anti, jnp.concatenate([nt(v0, d0), nt(v1, d1)], axis=1), 0.0).astype(BF)
        dq_in = nn(a, k_stack)
        dk_in = nn(a_t, q_stack)
        rin[:, at] = qc.astype(F32) * dq_in - kc.astype(F32) * dk_in
        dqi[:, at] = dqi[:, at] * dq_in
        dki[:, at] = dki[:, at] * dk_in
        dvi[:, values(c)] = jnp.concatenate(
            [nn(score_t[:, :tokens], d0), nn(score_t[:, tokens:], d1)], axis=1)

    latent_total = jnp.zeros((tokens, map_ref.shape[0]), F32)
    for c in range(pairs):
        at = lanes(c)
        state = s_in[c]
        costate = g_in[c]
        g_stack = stack(costate, low_state)
        dq_out = nn(do_ref[:, values(c)], stack(state, low_state))
        dk_out = nn(v_ref[:, values(c)], g_stack)
        dq_ref[:, at] = (dqi[:, at] + es[:, at] * dq_out).astype(BF)
        dk_ref[:, at] = (dki[:, at] + ee[:, at] * dk_out).astype(BF)
        dv_ref[:, values(c)] = (dvi[:, values(c)] + nt(ke[:, at], g_stack)).astype(BF)
        term = rin[:, at] + qs[:, at].astype(F32) * dq_out - ke[:, at].astype(F32) * dk_out
        leaving = dec[:, at] * state.astype(F32) + inc[c]
        carry = jnp.sum(leaving * costate.astype(F32), axis=0, keepdims=True)
        decay_grad = nn(suffix, thirds(term, 0)) + carry
        gate_grad = (decay_grad * gate[:, at]).astype(BF)
        latent_total = latent_total + nt(gate_grad, map_ref[:, at])
        dw = tn(latent, gate_grad)
        for p in range(n_sp):
            piece = dw[p * rows : (p + 1) * rows]
            w_own[p, :, at] = piece
            a_src[p, :, at] = piece.astype(BF)
    lg_ref[...] = latent_total.astype(BF)

    def a_copy(o):
        t = lax.rem(me + o, n_sp)
        return pltpu.make_async_remote_copy(
            src_ref=a_src.at[t], dst_ref=a_dst.at[o], send_sem=a_send.at[o], recv_sem=a_recv.at[o],
            device_id={"sp": t})

    def b_copy(o, slot):
        return pltpu.make_async_remote_copy(
            src_ref=b_all.at[mine], dst_ref=b_all.at[slot], send_sem=b_send.at[o], recv_sem=b_recv.at[o],
            device_id={"dp": lax.rem(mine + o, n_dp)})

    def c_copy(o, slot):
        return pltpu.make_async_remote_copy(
            src_ref=c_all.at[me], dst_ref=c_all.at[slot], send_sem=c_send.at[o], recv_sem=c_recv.at[o],
            device_id={"sp": lax.rem(me + o, n_sp)})

    for o in range(1, n_sp):
        a_copy(o).start()
    total = w_own[me]
    for o in range(1, n_sp):
        a_copy(o).wait_recv()
        total = total + a_dst[o].astype(F32)
    b_all[mine] = total.astype(BF)
    for o in range(1, n_dp):
        b_copy(o, mine).start()
    for o in range(1, n_dp):
        b_copy(o, lax.rem(mine + n_dp - o, n_dp)).wait_recv()
    total = b_all[0].astype(F32)
    for o in range(1, n_dp):
        total = total + b_all[o].astype(F32)
    c_all[me] = total.astype(BF)
    for o in range(1, n_sp):
        c_copy(o, me).start()
    for o in range(1, n_sp):
        c_copy(o, lax.rem(me + n_sp - o, n_sp)).wait_recv()
    for p in range(n_sp):
        wg_ref[p * rows : (p + 1) * rows, :] = c_all[p].astype(F32)

    for c in range(pairs):
        @pl.when(jnp.logical_not(last))
        def _():
            s_copy(c).wait_send()

        @pl.when(jnp.logical_not(first))
        def _():
            g_copy(c).wait_send()

    for o in range(1, n_sp):
        a_copy(o).wait_send()
        c_copy(o, me).wait_send()
    for o in range(1, n_dp):
        b_copy(o, mine).wait_send()


def solution(mesh):
    n_sp = mesh.shape["sp"]
    n_dp = mesh.shape["dp"]

    def on_device(q, k, v, do, latent, weight, bias, extra):
        tokens, width = q.shape
        rank = weight.shape[0]
        pairs = width // LANES
        vd = v.shape[1] // pairs // 2
        rows = rank // n_sp
        vmem = pl.BlockSpec(memory_space=pltpu.VMEM)
        wide = lambda kind: pltpu.VMEM((tokens, width), kind)
        state = lambda kind: pltpu.VMEM((pairs, vd, LANES), kind)
        sems = lambda n: pltpu.SemaphoreType.DMA((n,))
        return pl.pallas_call(
            functools.partial(kernel, n_sp, n_dp),
            out_shape=(
                jax.ShapeDtypeStruct(q.shape, BF),
                jax.ShapeDtypeStruct(k.shape, BF),
                jax.ShapeDtypeStruct(v.shape, BF),
                jax.ShapeDtypeStruct(latent.shape, BF),
                jax.ShapeDtypeStruct(weight.shape, F32),
            ),
            in_specs=[vmem] * 8,
            out_specs=(vmem,) * 5,
            scratch_shapes=[
                wide(BF), wide(BF), wide(BF), wide(BF), wide(F32), wide(F32), wide(F32),
                pltpu.VMEM((1, width), F32), state(F32), state(F32),
                wide(F32), wide(F32), pltpu.VMEM(v.shape, F32), wide(F32),
                state(BF), state(BF), state(BF), state(BF),
                pltpu.VMEM((n_sp, rows, width), F32), pltpu.VMEM((n_sp, rows, width), BF),
                pltpu.VMEM((n_sp, rows, width), BF), pltpu.VMEM((n_dp, rows, width), BF),
                pltpu.VMEM((n_sp, rows, width), BF),
                sems(pairs), sems(pairs), sems(pairs), sems(pairs),
                sems(n_sp), sems(n_sp), sems(n_dp), sems(n_dp), sems(n_sp), sems(n_sp),
            ],
            compiler_params=pltpu.CompilerParams(
                collective_id=0, has_side_effects=True, vmem_limit_bytes=48 * 1024 * 1024),
            name="gla_backward",
        )(q, k, v, do, latent, weight, bias.reshape(1, -1), extra)

    tokens = P(("dp", "sp"), None)
    return jax.shard_map(
        on_device,
        mesh=mesh,
        in_specs=(tokens,) * 5 + (P(), P(), tokens),
        out_specs=(tokens,) * 4 + (P(),),
        check_vma=False,
    )
```

time: 279 us -> 89.4 us (0.32)
  Pallas kernels: 0 us -> 78.4 us
  waiting for transfers between devices: 67.7 us -> 0 us
  other arithmetic: 56 us -> 0 us
  starting transfers between devices: 38 us -> 0 us
  matrix products: 32.9 us -> 0 us
  local copies, waits for them, and re-layouts: 39.8 us -> 10 us
  blocking collectives: 26.6 us -> 0 us
  between operations: 15.9 us -> 0.67 us
    pallas_call x0 -> x1, Pallas kernels: none -> 78.4 us  [on_device(): pl.pallas_call(functools.partial(kernel, n_sp, n_dp), out_shape=(jax.Shap...]
    psum x1 -> x0, waiting for transfers between devices: 56.5 us -> none  [on_device(): summed = lax.psum(local_weight, 'dp')]
    another operation x4 -> x0, other arithmetic: 53.1 us -> none  [the longest x2 51.6 us: gla_forward(): cumulative = jnp.cumsum(blocked(logarithm_decay), axis=2)]
    all_to_all x8 -> x0, starting transfers between devices: 37.9 us -> none  [the longest x1 6.49 us: on_device(): lax.all_to_all(surplus_damping, 'sp', split_axis=1, concat_axis=0, tiled=...]
    dot_general x16 -> x0, matrix products: 32.9 us -> none  [the longest x3 9.75 us: carry_states(): return jnp.einsum('hnmk,mhkv->nhkv', weights, increments, precision=highest)]
    all_gather x2 -> x0, blocking collectives: 26.6 us -> none  [the longest x1 14.1 us: on_device(): weight_grad = lax.all_gather(summed, 'sp', axis=1, tiled=True)]
    all_to_all x8 -> x0, waiting for transfers between devices: 11.2 us -> none  [the longest x1 7.02 us: on_device(): lax.all_to_all(probe_vectors, 'sp', split_axis=1, concat_axis=0, tiled=True)]
    convert_element_type x10 -> x0, local copies, waits for them, and re-layouts: 7.84 us -> none  [the longest x4 4.98 us: on_device(): to_rows(grad_query).astype(jnp.bfloat16)]
  transfers between devices with their start and end apart: 10 -> 0, of which waited for: 4 -> 0; matrix products, arithmetic and copies ran while one was open for 31% -> 0% of each run, Pallas kernels for 0% -> 0%
where the time goes in v1:
time: 89.4 us; the launch traced here: 89 us
  Pallas kernels  78.4 us (88%)
  local copies, waits for them, and re-layouts  10 us (11%)
    pallas_call x1, Pallas kernels, on_device(): pl.pallas_call(functools.partial(kernel, n_sp, n_dp), out_shape=(jax.Shap...  78.4 us
    unnamed x20, local copies, waits for them, and re-layouts  9.3 us

profile of v1, /device:TPU:0, one launch (start us, length us, event | category | flops | bytes accessed | tf_op | source)
XLA Modules:
  0.0 89.0 jit_solution(7201527946533494622)
XLA Ops:
  0.6 0.0 copy-start.6
  0.6 0.8 copy.13.lat_ref
  1.5 0.0 copy-done.6
  1.5 0.0 copy-start.5
  1.5 0.1 copy.14.extra_ref
  1.6 0.6 copy-done.5
  2.2 0.0 copy-start
  2.2 1.0 %copy-done = bf16[128,2048]{1,0:T(8,128)(2,1)S(1)} copy-done((bf16[128,2048]{1,0:T(8,128)(2,1)S(1)}, bf16[128,2048]{1,0:T(8,128)(2,1)}, u32[]{:S(2)}) %copy-start) | copy-done | bytes 524312
  3.2 0.0 copy-start.1
  3.2 1.0 %copy-done.1 = bf16[128,2048]{1,0:T(8,128)(2,1)S(1)} copy-done((bf16[128,2048]{1,0:T(8,128)(2,1)S(1)}, bf16[128,2048]{1,0:T(8,128)(2,1)}, u32[]{:S(2)}) %copy-start.1) | copy-done | bytes 524312
  4.3 0.0 copy-start.2
  4.3 0.9 %copy-done.2 = bf16[128,1024]{1,0:T(8,128)(2,1)S(1)} copy-done((bf16[128,1024]{1,0:T(8,128)(2,1)S(1)}, bf16[128,1024]{1,0:T(8,128)(2,1)}, u32[]{:S(2)}) %copy-start.2) | copy-done | bytes 262168
  5.2 0.0 copy-start.3
  5.2 0.9 %copy-done.3 = bf16[128,1024]{1,0:T(8,128)(2,1)S(1)} copy-done((bf16[128,1024]{1,0:T(8,128)(2,1)S(1)}, bf16[128,1024]{1,0:T(8,128)(2,1)}, u32[]{:S(2)}) %copy-start.3) | copy-done | bytes 262168
  6.2 0.0 copy-start.4
  6.2 0.9 %copy-done.4 = bf16[64,1024]{1,0:T(8,128)(2,1)S(1)} copy-done((bf16[64,1024]{1,0:T(8,128)(2,1)S(1)}, bf16[64,1024]{1,0:T(8,128)(2,1)}, u32[]{:S(2)}) %copy-start.4) | copy-done | bytes 131096
  7.1 78.4 %gla_backward.1 = (bf16[128,1024]{1,0:T(8,128)(2,1)S(1)}, bf16[128,1024]{1,0:T(8,128)(2,1)S(1)}, bf16[128,2048]{1,0:T(8,128)(2,1)S(1)}, bf16[128,64]{1,0:T(8,128)(2,1)S(1)}, f32[64,1024]{1,0:T(8,128)S(1)}) custom-call(bf16[128,1024]{1,0:T(8,128)(2,1)S(1)} %copy-done.2, bf16[128,1024]{1,0:T(8,128)(2,1)S(1)} %copy-done.3, bf16[128,2048]{1,0:T(8,128)(2,1)S(1)} %copy-done, ...), custom_call_target="tpu_custom_call" | custom-call | tf_op jit(solution)/shard_map/gla_backward/pallas_call | solution.py:288
  85.4 0.7 copy.15
  86.1 0.7 copy.20
  86.8 0.7 copy.21
  87.5 0.8 copy.22
  88.3 0.7 copy.23
Async XLA Ops:
  0.6 0.8 copy-start.6
  1.5 0.7 copy-start.5
  2.2 1.0 %copy-start = (bf16[128,2048]{1,0:T(8,128)(2,1)S(1)}, bf16[128,2048]{1,0:T(8,128)(2,1)}, u32[]{:S(2)}) copy-start(bf16[128,2048]{1,0:T(8,128)(2,1)} %v_ref.1) | copy-start | bytes 1572868
  3.2 1.0 %copy-start.1 = (bf16[128,2048]{1,0:T(8,128)(2,1)S(1)}, bf16[128,2048]{1,0:T(8,128)(2,1)}, u32[]{:S(2)}) copy-start(bf16[128,2048]{1,0:T(8,128)(2,1)} %do_ref.1) | copy-start | bytes 1572868
  4.3 0.9 %copy-start.2 = (bf16[128,1024]{1,0:T(8,128)(2,1)S(1)}, bf16[128,1024]{1,0:T(8,128)(2,1)}, u32[]{:S(2)}) copy-start(bf16[128,1024]{1,0:T(8,128)(2,1)} %q_ref.1) | copy-start | bytes 786436
  5.2 0.9 %copy-start.3 = (bf16[128,1024]{1,0:T(8,128)(2,1)S(1)}, bf16[128,1024]{1,0:T(8,128)(2,1)}, u32[]{:S(2)}) copy-start(bf16[128,1024]{1,0:T(8,128)(2,1)} %k_ref.1) | copy-start | bytes 786436
  6.2 0.9 %copy-start.4 = (bf16[64,1024]{1,0:T(8,128)(2,1)S(1)}, bf16[64,1024]{1,0:T(8,128)(2,1)}, u32[]{:S(2)}) copy-start(bf16[64,1024]{1,0:T(8,128)(2,1)} %map_ref.1) | copy-start | bytes 393220

commit v2 on v1

--- a/solution.py
+++ b/solution.py
@@ -35,15 +35,16 @@
 
 def kernel(
     n_sp, n_dp,
-    q_ref, k_ref, v_ref, do_ref, lat_ref, map_ref, bias_ref, extra_ref,
+    q_hbm, k_hbm, v_hbm, do_hbm, lat_hbm, map_hbm, bias_hbm, extra_hbm,
     dq_ref, dk_ref, dv_ref, lg_ref, wg_ref,
+    q_ref, k_ref, v_ref, do_ref, lat_ref, map_ref, bias_ref, extra_ref, in_sem,
     qd, kd, qs, ke, es, ee, gate, dec, inc, adj, dqi, dki, dvi, rin,
     s_in, s_out, g_in, g_out,
     w_own, a_src, a_dst, b_all, c_all,
     s_send, s_recv, g_send, g_recv, a_send, a_recv, b_send, b_recv, c_send, c_recv,
 ):
     tokens, width = q_ref.shape
-    heads = extra_ref.shape[1]
+    heads = extra_ref.shape[0]
     key_width = width // heads
     pairs = width // LANES
     value_width = v_ref.shape[1] // pairs
@@ -55,6 +56,12 @@
     mine = lax.axis_index("dp")
     first = me == 0
     last = me == n_sp - 1
+
+    sources = (lat_hbm, extra_hbm, map_hbm, bias_hbm, k_hbm, q_hbm, v_hbm, do_hbm)
+    targets = (lat_ref, extra_ref, map_ref, bias_ref, k_ref, q_ref, v_ref, do_ref)
+    loads = [pltpu.make_async_copy(a, b, in_sem.at[n]) for n, (a, b) in enumerate(zip(sources, targets))]
+    for load in loads:
+        load.start()
 
     barrier = pltpu.get_barrier_semaphore()
     for o in range(1, n_sp):
@@ -95,8 +102,11 @@
             src_ref=g_out.at[c], dst_ref=g_in.at[c], send_sem=g_send.at[c], recv_sem=g_recv.at[c],
             device_id={"sp": lax.rem(me + n_sp - 1, n_sp)})
 
-    latent = lat_ref[...]
-    extra = extra_ref[...]
+    for load in loads:
+        load.wait()
+    latent_t = lat_ref[...]
+    latent = latent_t.astype(F32).T.astype(BF)
+    extra = extra_ref[...].astype(F32).T.astype(BF)
     pl.semaphore_wait(barrier, n_sp + n_dp - 2)
 
     @pl.when(first)
@@ -152,28 +162,24 @@
             g_out[c] = adjoint.astype(BF)
             g_copy(c).start()
 
-    inner = jnp.logical_and(jnp.logical_not(first), jnp.logical_not(last))
-    for c in range(pairs):
+    def relay_s(c):
+        s_copy(c).wait_recv()
+
+        @pl.when(jnp.logical_not(last))
+        def _():
+            s_out[c] = (dec[:, lanes(c)] * s_in[c].astype(F32) + inc[c]).astype(BF)
+            s_copy(c).start()
+
+    def relay_g(c):
+        g_copy(c).wait_recv()
+
+        @pl.when(jnp.logical_not(first))
+        def _():
+            g_out[c] = (dec[:, lanes(c)] * g_in[c].astype(F32) + adj[c]).astype(BF)
+            g_copy(c).start()
+
+    def inside(c):
         at = lanes(c)
-
-        @pl.when(jnp.logical_not(first))
-        def _():
-            s_copy(c).wait_recv()
-
-        @pl.when(inner)
-        def _():
-            s_out[c] = (dec[:, at] * s_in[c].astype(F32) + inc[c]).astype(BF)
-            s_copy(c).start()
-
-        @pl.when(jnp.logical_not(last))
-        def _():
-            g_copy(c).wait_recv()
-
-        @pl.when(inner)
-        def _():
-            g_out[c] = (dec[:, at] * g_in[c].astype(F32) + adj[c]).astype(BF)
-            g_copy(c).start()
-
         qc = qd[:, at]
         kc = kd[:, at]
         q_stack = stack(qc, low_lane)
@@ -193,7 +199,32 @@
         dvi[:, values(c)] = jnp.concatenate(
             [nn(score_t[:, :tokens], d0), nn(score_t[:, tokens:], d1)], axis=1)
 
-    latent_total = jnp.zeros((tokens, map_ref.shape[0]), F32)
+    lead = pairs // 2
+    left = me < n_sp // 2
+    for c in range(lead):
+        inside(c)
+    for step in range(pairs + lead):
+        if step < pairs:
+            @pl.when(jnp.logical_and(left, jnp.logical_not(first)))
+            def _():
+                relay_s(step)
+
+            @pl.when(jnp.logical_not(jnp.logical_or(left, last)))
+            def _():
+                relay_g(step)
+
+            if step >= lead:
+                inside(step)
+        if step >= lead:
+            @pl.when(left)
+            def _():
+                relay_g(step - lead)
+
+            @pl.when(jnp.logical_not(left))
+            def _():
+                relay_s(step - lead)
+
+    latent_total = jnp.zeros((map_ref.shape[0], tokens), F32)
     for c in range(pairs):
         at = lanes(c)
         state = s_in[c]
@@ -209,8 +240,8 @@
         carry = jnp.sum(leaving * costate.astype(F32), axis=0, keepdims=True)
         decay_grad = nn(suffix, thirds(term, 0)) + carry
         gate_grad = (decay_grad * gate[:, at]).astype(BF)
-        latent_total = latent_total + nt(gate_grad, map_ref[:, at])
-        dw = tn(latent, gate_grad)
+        latent_total = latent_total + nt(map_ref[:, at], gate_grad)
+        dw = nn(latent_t, gate_grad)
         for p in range(n_sp):
             piece = dw[p * rows : (p + 1) * rows]
             w_own[p, :, at] = piece
@@ -285,18 +316,21 @@
         wide = lambda kind: pltpu.VMEM((tokens, width), kind)
         state = lambda kind: pltpu.VMEM((pairs, vd, LANES), kind)
         sems = lambda n: pltpu.SemaphoreType.DMA((n,))
-        return pl.pallas_call(
+        grads = pl.pallas_call(
             functools.partial(kernel, n_sp, n_dp),
             out_shape=(
                 jax.ShapeDtypeStruct(q.shape, BF),
                 jax.ShapeDtypeStruct(k.shape, BF),
                 jax.ShapeDtypeStruct(v.shape, BF),
-                jax.ShapeDtypeStruct(latent.shape, BF),
+                jax.ShapeDtypeStruct(latent.shape[::-1], BF),
                 jax.ShapeDtypeStruct(weight.shape, F32),
             ),
-            in_specs=[vmem] * 8,
+            in_specs=[pl.BlockSpec(memory_space=pltpu.HBM)] * 8,
             out_specs=(vmem,) * 5,
             scratch_shapes=[
+                pltpu.VMEM(q.shape, BF), pltpu.VMEM(k.shape, BF), pltpu.VMEM(v.shape, BF), pltpu.VMEM(do.shape, BF),
+                pltpu.VMEM(latent.shape[::-1], BF), pltpu.VMEM(weight.shape, BF),
+                pltpu.VMEM((1, width), F32), pltpu.VMEM(extra.shape[::-1], BF), sems(8),
                 wide(BF), wide(BF), wide(BF), wide(BF), wide(F32), wide(F32), wide(F32),
                 pltpu.VMEM((1, width), F32), state(F32), state(F32),
                 wide(F32), wide(F32), pltpu.VMEM(v.shape, F32), wide(F32),
@@ -310,7 +344,8 @@
             compiler_params=pltpu.CompilerParams(
                 collective_id=0, has_side_effects=True, vmem_limit_bytes=48 * 1024 * 1024),
             name="gla_backward",
-        )(q, k, v, do, latent, weight, bias.reshape(1, -1), extra)
+        )(q, k, v, do, latent.T, weight, bias.reshape(1, -1), extra.T)
+        return grads[0], grads[1], grads[2], grads[3].T, grads[4]
 
     tokens = P(("dp", "sp"), None)
     return jax.shard_map(

time: 89.4 us -> 49.5 us (0.55)
  Pallas kernels: 78.4 us -> 38 us
    pallas_call x1, Pallas kernels: 78.4 us -> 38 us  [on_device(): pl.pallas_call(functools.partial(kernel, n_sp, n_dp), out_shape=(jax.Shap...]
    unnamed x20 -> x21, local copies, waits for them, and re-layouts: 9.3 us -> 10.5 us
where the time goes in v2:
time: 49.5 us; the launch traced here: 49.1 us
  Pallas kernels  38 us (77%)
  local copies, waits for them, and re-layouts  10.5 us (21%)
  between operations  0.66 us (1%)
    pallas_call x1, Pallas kernels, on_device(): pl.pallas_call(functools.partial(kernel, n_sp, n_dp), out_shape=(jax.Shap...  38 us
    unnamed x21, local copies, waits for them, and re-layouts  10.5 us

profile of v2, /device:TPU:0, one launch (start us, length us, event | category | flops | bytes accessed | tf_op | source)
XLA Modules:
  0.0 49.1 jit_solution(8505855566232128649)
XLA Ops:
  0.6 0.0 copy-start.6
  0.6 0.7 %copy-done.6 = f32[1024]{0:T(1024)S(1)} copy-done((f32[1024]{0:T(1024)S(1)}, f32[1024]{0:T(1024)}, u32[]{:S(2)}) %copy-start.6) | copy-done | bytes 4120
  1.3 0.0 copy-start
  1.3 1.0 %copy-done = bf16[128,2048]{1,0:T(8,128)(2,1)S(1)} copy-done((bf16[128,2048]{1,0:T(8,128)(2,1)S(1)}, bf16[128,2048]{1,0:T(8,128)(2,1)}, u32[]{:S(2)}) %copy-start) | copy-done | bytes 524312
  2.4 0.0 copy-start.1
  2.4 1.0 %copy-done.1 = bf16[128,2048]{1,0:T(8,128)(2,1)S(1)} copy-done((bf16[128,2048]{1,0:T(8,128)(2,1)S(1)}, bf16[128,2048]{1,0:T(8,128)(2,1)}, u32[]{:S(2)}) %copy-start.1) | copy-done | bytes 524312
  3.4 0.0 copy-start.2
  3.4 0.9 %copy-done.2 = bf16[128,1024]{1,0:T(8,128)(2,1)S(1)} copy-done((bf16[128,1024]{1,0:T(8,128)(2,1)S(1)}, bf16[128,1024]{1,0:T(8,128)(2,1)}, u32[]{:S(2)}) %copy-start.2) | copy-done | bytes 262168
  4.4 0.0 copy-start.3
  4.4 0.9 %copy-done.3 = bf16[128,1024]{1,0:T(8,128)(2,1)S(1)} copy-done((bf16[128,1024]{1,0:T(8,128)(2,1)S(1)}, bf16[128,1024]{1,0:T(8,128)(2,1)}, u32[]{:S(2)}) %copy-start.3) | copy-done | bytes 262168
  5.3 0.0 copy-start.4
  5.3 0.9 %copy-done.4 = bf16[64,1024]{1,0:T(8,128)(2,1)S(1)} copy-done((bf16[64,1024]{1,0:T(8,128)(2,1)S(1)}, bf16[64,1024]{1,0:T(8,128)(2,1)}, u32[]{:S(2)}) %copy-start.4) | copy-done | bytes 131096
  6.2 0.0 copy-start.5
  6.2 0.7 %copy-done.5 = bf16[128,64]{0,1:T(8,128)(2,1)S(1)} copy-done((bf16[128,64]{0,1:T(8,128)(2,1)S(1)}, bf16[128,64]{0,1:T(8,128)(2,1)}, u32[]{:S(2)}) %copy-start.5) | copy-done | bytes 16408
  6.9 0.0 copy-start.7
  6.9 0.7 %copy-done.7 = bf16[128,16]{0,1:T(8,128)(2,1)S(1)} copy-done((bf16[128,16]{0,1:T(8,128)(2,1)S(1)}, bf16[128,16]{0,1:T(8,128)(2,1)}, u32[]{:S(2)}) %copy-start.7) | copy-done | bytes 4120
  7.6 38.0 %gla_backward.1 = (bf16[128,1024]{1,0:T(8,128)(2,1)S(1)}, bf16[128,1024]{1,0:T(8,128)(2,1)S(1)}, bf16[128,2048]{1,0:T(8,128)(2,1)S(1)}, bf16[64,128]{1,0:T(8,128)(2,1)S(1)}, f32[64,1024]{1,0:T(8,128)S(1)}) custom-call(bf16[128,1024]{1,0:T(8,128)(2,1)S(1)} %copy-done.2, bf16[128,1024]{1,0:T(8,128)(2,1)S(1)} %copy-done.3, bf16[128,2048]{1,0:T(8,128)(2,1)S(1)} %copy-done, ...), custom_call_target="tpu_custom_call" | custom-call | tf_op jit(solution)/shard_map/gla_backward/pallas_call | solution.py:319
  45.6 0.7 %copy.18 = bf16[128,1024]{1,0:T(8,128)(2,1)} copy(bf16[128,1024]{1,0:T(8,128)(2,1)S(1)} %get-tuple-element.20) | data formatting | bytes 524288
  46.3 0.7 %copy.19 = bf16[128,1024]{1,0:T(8,128)(2,1)} copy(bf16[128,1024]{1,0:T(8,128)(2,1)S(1)} %get-tuple-element.21) | data formatting | bytes 524288
  47.0 0.8 %copy.20 = bf16[128,2048]{1,0:T(8,128)(2,1)} copy(bf16[128,2048]{1,0:T(8,128)(2,1)S(1)} %get-tuple-element.22) | data formatting | bytes 1048576
  47.8 0.6 %copy.21 = bf16[128,64]{0,1:T(8,128)(2,1)} copy(bf16[128,64]{0,1:T(8,128)(2,1)S(1)} %bitcast.5) | data formatting | bytes 32768
  48.4 0.7 %copy.22 = f32[64,1024]{1,0:T(8,128)} copy(f32[64,1024]{1,0:T(8,128)S(1)} %get-tuple-element.24) | data formatting | bytes 524288
Async XLA Ops:
  0.6 0.7 %copy-start.6 = (f32[1024]{0:T(1024)S(1)}, f32[1024]{0:T(1024)}, u32[]{:S(2)}) copy-start(f32[1024]{0:T(1024)} %param.14) | copy-start | bytes 12292
  1.3 1.0 %copy-start = (bf16[128,2048]{1,0:T(8,128)(2,1)S(1)}, bf16[128,2048]{1,0:T(8,128)(2,1)}, u32[]{:S(2)}) copy-start(bf16[128,2048]{1,0:T(8,128)(2,1)} %v_hbm.1) | copy-start | bytes 1572868
  2.4 1.0 %copy-start.1 = (bf16[128,2048]{1,0:T(8,128)(2,1)S(1)}, bf16[128,2048]{1,0:T(8,128)(2,1)}, u32[]{:S(2)}) copy-start(bf16[128,2048]{1,0:T(8,128)(2,1)} %do_hbm.1) | copy-start | bytes 1572868
  3.4 0.9 %copy-start.2 = (bf16[128,1024]{1,0:T(8,128)(2,1)S(1)}, bf16[128,1024]{1,0:T(8,128)(2,1)}, u32[]{:S(2)}) copy-start(bf16[128,1024]{1,0:T(8,128)(2,1)} %q_hbm.1) | copy-start | bytes 786436
  4.4 0.9 %copy-start.3 = (bf16[128,1024]{1,0:T(8,128)(2,1)S(1)}, bf16[128,1024]{1,0:T(8,128)(2,1)}, u32[]{:S(2)}) copy-start(bf16[128,1024]{1,0:T(8,128)(2,1)} %k_hbm.1) | copy-start | bytes 786436
  5.3 0.9 %copy-start.4 = (bf16[64,1024]{1,0:T(8,128)(2,1)S(1)}, bf16[64,1024]{1,0:T(8,128)(2,1)}, u32[]{:S(2)}) copy-start(bf16[64,1024]{1,0:T(8,128)(2,1)} %map_hbm.1) | copy-start | bytes 393220
  6.2 0.7 %copy-start.5 = (bf16[128,64]{0,1:T(8,128)(2,1)S(1)}, bf16[128,64]{0,1:T(8,128)(2,1)}, u32[]{:S(2)}) copy-start(bf16[128,64]{0,1:T(8,128)(2,1)} %param.12) | copy-start | bytes 49156
  6.9 0.7 %copy-start.7 = (bf16[128,16]{0,1:T(8,128)(2,1)S(1)}, bf16[128,16]{0,1:T(8,128)(2,1)}, u32[]{:S(2)}) copy-start(bf16[128,16]{0,1:T(8,128)(2,1)} %param.15) | copy-start | bytes 12292

commit v3 on v2

--- a/solution.py
+++ b/solution.py
@@ -11,6 +11,7 @@
 BF = jnp.bfloat16
 F32 = jnp.float32
 LANES = 128
+HALVES = 2
 
 
 def nn(a, b):
@@ -107,7 +108,6 @@
     latent_t = lat_ref[...]
     latent = latent_t.astype(F32).T.astype(BF)
     extra = extra_ref[...].astype(F32).T.astype(BF)
-    pl.semaphore_wait(barrier, n_sp + n_dp - 2)
 
     @pl.when(first)
     def _():
@@ -151,6 +151,8 @@
         adjoint = jnp.where(low_state, both[:vd], both[vd:])
         inc[c] = increment
         adj[c] = adjoint
+        if c == 0:
+            pl.semaphore_wait(barrier, n_sp + n_dp - 2)
 
         @pl.when(first)
         def _():
@@ -199,34 +201,30 @@
         dvi[:, values(c)] = jnp.concatenate(
             [nn(score_t[:, :tokens], d0), nn(score_t[:, tokens:], d1)], axis=1)
 
-    lead = pairs // 2
-    left = me < n_sp // 2
-    for c in range(lead):
-        inside(c)
-    for step in range(pairs + lead):
-        if step < pairs:
-            @pl.when(jnp.logical_and(left, jnp.logical_not(first)))
-            def _():
-                relay_s(step)
-
-            @pl.when(jnp.logical_not(jnp.logical_or(left, last)))
-            def _():
-                relay_g(step)
-
-            if step >= lead:
-                inside(step)
-        if step >= lead:
-            @pl.when(left)
-            def _():
-                relay_g(step - lead)
-
-            @pl.when(jnp.logical_not(left))
-            def _():
-                relay_s(step - lead)
-
-    latent_total = jnp.zeros((map_ref.shape[0], tokens), F32)
-    for c in range(pairs):
+    lead = pairs // HALVES
+
+    def a_copy(h, o):
+        t = lax.rem(me + o, n_sp)
+        return pltpu.make_async_remote_copy(
+            src_ref=a_src.at[h, t], dst_ref=a_dst.at[h, o], send_sem=a_send.at[h, o],
+            recv_sem=a_recv.at[h, o], device_id={"sp": t})
+
+    def b_copy(h, o, slot):
+        return pltpu.make_async_remote_copy(
+            src_ref=b_all.at[h, mine], dst_ref=b_all.at[h, slot], send_sem=b_send.at[h, o],
+            recv_sem=b_recv.at[h, o], device_id={"dp": lax.rem(mine + o, n_dp)})
+
+    def c_copy(h, o, slot):
+        return pltpu.make_async_remote_copy(
+            src_ref=c_all.at[h, me], dst_ref=c_all.at[h, slot], send_sem=c_send.at[h, o],
+            recv_sem=c_recv.at[h, o], device_id={"sp": lax.rem(me + o, n_sp)})
+
+
+    latent_parts = []
+
+    def final(c):
         at = lanes(c)
+        here = lanes(c % lead)
         state = s_in[c]
         costate = g_in[c]
         g_stack = stack(costate, low_state)
@@ -240,51 +238,68 @@
         carry = jnp.sum(leaving * costate.astype(F32), axis=0, keepdims=True)
         decay_grad = nn(suffix, thirds(term, 0)) + carry
         gate_grad = (decay_grad * gate[:, at]).astype(BF)
-        latent_total = latent_total + nt(map_ref[:, at], gate_grad)
+        latent_parts.append(nt(map_ref[:, at], gate_grad))
         dw = nn(latent_t, gate_grad)
         for p in range(n_sp):
             piece = dw[p * rows : (p + 1) * rows]
-            w_own[p, :, at] = piece
-            a_src[p, :, at] = piece.astype(BF)
-    lg_ref[...] = latent_total.astype(BF)
-
-    def a_copy(o):
-        t = lax.rem(me + o, n_sp)
-        return pltpu.make_async_remote_copy(
-            src_ref=a_src.at[t], dst_ref=a_dst.at[o], send_sem=a_send.at[o], recv_sem=a_recv.at[o],
-            device_id={"sp": t})
-
-    def b_copy(o, slot):
-        return pltpu.make_async_remote_copy(
-            src_ref=b_all.at[mine], dst_ref=b_all.at[slot], send_sem=b_send.at[o], recv_sem=b_recv.at[o],
-            device_id={"dp": lax.rem(mine + o, n_dp)})
-
-    def c_copy(o, slot):
-        return pltpu.make_async_remote_copy(
-            src_ref=c_all.at[me], dst_ref=c_all.at[slot], send_sem=c_send.at[o], recv_sem=c_recv.at[o],
-            device_id={"sp": lax.rem(me + o, n_sp)})
-
-    for o in range(1, n_sp):
-        a_copy(o).start()
-    total = w_own[me]
-    for o in range(1, n_sp):
-        a_copy(o).wait_recv()
-        total = total + a_dst[o].astype(F32)
-    b_all[mine] = total.astype(BF)
-    for o in range(1, n_dp):
-        b_copy(o, mine).start()
-    for o in range(1, n_dp):
-        b_copy(o, lax.rem(mine + n_dp - o, n_dp)).wait_recv()
-    total = b_all[0].astype(F32)
-    for o in range(1, n_dp):
-        total = total + b_all[o].astype(F32)
-    c_all[me] = total.astype(BF)
-    for o in range(1, n_sp):
-        c_copy(o, me).start()
-    for o in range(1, n_sp):
-        c_copy(o, lax.rem(me + n_sp - o, n_sp)).wait_recv()
-    for p in range(n_sp):
-        wg_ref[p * rows : (p + 1) * rows, :] = c_all[p].astype(F32)
+            w_own[c // lead, p, :, here] = piece
+            a_src[c // lead, p, :, here] = piece.astype(BF)
+
+    left = me < n_sp // 2
+    for c in range(lead):
+        inside(c)
+    for step in range(pairs + lead):
+        if step < pairs:
+            @pl.when(jnp.logical_and(left, jnp.logical_not(first)))
+            def _():
+                relay_s(step)
+
+            @pl.when(jnp.logical_not(jnp.logical_or(left, last)))
+            def _():
+                relay_g(step)
+
+            if step >= lead:
+                inside(step)
+        if step >= lead:
+            @pl.when(left)
+            def _():
+                relay_g(step - lead)
+
+            @pl.when(jnp.logical_not(left))
+            def _():
+                relay_s(step - lead)
+
+            final(step - lead)
+            if (step + 1) % lead == 0:
+                for o in range(1, n_sp):
+                    a_copy(step // lead - 1, o).start()
+
+    lg_ref[...] = functools.reduce(jnp.add, latent_parts).astype(BF)
+
+    halves = range(HALVES)
+    for h in halves:
+        total = w_own[h, me]
+        for o in range(1, n_sp):
+            a_copy(h, o).wait_recv()
+            total = total + a_dst[h, o].astype(F32)
+        b_all[h, mine] = total.astype(BF)
+        for o in range(1, n_dp):
+            b_copy(h, o, mine).start()
+    for h in halves:
+        for o in range(1, n_dp):
+            b_copy(h, o, lax.rem(mine + n_dp - o, n_dp)).wait_recv()
+        total = b_all[h, 0].astype(F32)
+        for o in range(1, n_dp):
+            total = total + b_all[h, o].astype(F32)
+        c_all[h, me] = total.astype(BF)
+        for o in range(1, n_sp):
+            c_copy(h, o, me).start()
+    for h in halves:
+        for o in range(1, n_sp):
+            c_copy(h, o, lax.rem(me + n_sp - o, n_sp)).wait_recv()
+        half = wg_ref.shape[1] // HALVES
+        for p in range(n_sp):
+            wg_ref[p * rows : (p + 1) * rows, h * half : (h + 1) * half] = c_all[h, p].astype(F32)
 
     for c in range(pairs):
         @pl.when(jnp.logical_not(last))
@@ -295,11 +310,34 @@
         def _():
             g_copy(c).wait_send()
 
-    for o in range(1, n_sp):
-        a_copy(o).wait_send()
-        c_copy(o, me).wait_send()
-    for o in range(1, n_dp):
-        b_copy(o, mine).wait_send()
+    for h in halves:
+        for o in range(1, n_sp):
+            a_copy(h, o).wait_send()
+            c_copy(h, o, me).wait_send()
+        for o in range(1, n_dp):
+            b_copy(h, o, mine).wait_send()
+
+
+def writer(*refs):
+    n = len(refs) // 2
+    sem = refs[-1]
+    copies = [pltpu.make_async_copy(a, b, sem.at[i]) for i, (a, b) in enumerate(zip(refs[:n], refs[n:-1]))]
+    for copy in copies:
+        copy.start()
+    for copy in copies:
+        copy.wait()
+
+
+def write_out(arrays):
+    hbm = pl.BlockSpec(memory_space=pltpu.HBM)
+    return pl.pallas_call(
+        writer,
+        out_shape=tuple(jax.ShapeDtypeStruct(a.shape, a.dtype) for a in arrays),
+        in_specs=[pl.BlockSpec(memory_space=pltpu.VMEM)] * len(arrays),
+        out_specs=(hbm,) * len(arrays),
+        scratch_shapes=[pltpu.SemaphoreType.DMA((len(arrays),))],
+        name="write_out",
+    )(*arrays)
 
 
 def solution(mesh):
@@ -316,6 +354,7 @@
         wide = lambda kind: pltpu.VMEM((tokens, width), kind)
         state = lambda kind: pltpu.VMEM((pairs, vd, LANES), kind)
         sems = lambda n: pltpu.SemaphoreType.DMA((n,))
+        halves = lambda n: pltpu.SemaphoreType.DMA((HALVES, n))
         grads = pl.pallas_call(
             functools.partial(kernel, n_sp, n_dp),
             out_shape=(
@@ -335,16 +374,17 @@
                 pltpu.VMEM((1, width), F32), state(F32), state(F32),
                 wide(F32), wide(F32), pltpu.VMEM(v.shape, F32), wide(F32),
                 state(BF), state(BF), state(BF), state(BF),
-                pltpu.VMEM((n_sp, rows, width), F32), pltpu.VMEM((n_sp, rows, width), BF),
-                pltpu.VMEM((n_sp, rows, width), BF), pltpu.VMEM((n_dp, rows, width), BF),
-                pltpu.VMEM((n_sp, rows, width), BF),
+                pltpu.VMEM((HALVES, n_sp, rows, width // HALVES), F32), pltpu.VMEM((HALVES, n_sp, rows, width // HALVES), BF),
+                pltpu.VMEM((HALVES, n_sp, rows, width // HALVES), BF), pltpu.VMEM((HALVES, n_dp, rows, width // HALVES), BF),
+                pltpu.VMEM((HALVES, n_sp, rows, width // HALVES), BF),
                 sems(pairs), sems(pairs), sems(pairs), sems(pairs),
-                sems(n_sp), sems(n_sp), sems(n_dp), sems(n_dp), sems(n_sp), sems(n_sp),
+                halves(n_sp), halves(n_sp), halves(n_dp), halves(n_dp), halves(n_sp), halves(n_sp),
             ],
             compiler_params=pltpu.CompilerParams(
-                collective_id=0, has_side_effects=True, vmem_limit_bytes=48 * 1024 * 1024),
+                collective_id=0, has_side_effects=True, vmem_limit_bytes=67043328),
             name="gla_backward",
         )(q, k, v, do, latent.T, weight, bias.reshape(1, -1), extra.T)
+        grads = write_out(grads)
         return grads[0], grads[1], grads[2], grads[3].T, grads[4]
 
     tokens = P(("dp", "sp"), None)

time: 49.5 us -> 39.7 us (0.80)
  local copies, waits for them, and re-layouts: 10.5 us -> 0 us
  Pallas kernels: 38 us -> 38.9 us
    unnamed x21 -> x0, local copies, waits for them, and re-layouts: 10.5 us -> none
    pallas_call x0 -> x1, Pallas kernels: none -> 2.38 us  [write_out(): pl.pallas_call(writer, out_shape=tuple((jax.ShapeDtypeStruct(a.shape, a.d...]
    pallas_call x1, Pallas kernels: 38 us -> 36.5 us  [on_device(): pl.pallas_call(functools.partial(kernel, n_sp, n_dp), out_shape=(jax.Shap...]
where the time goes in v3:
time: 39.7 us; the launch traced here: 39.5 us
  Pallas kernels  38.9 us (98%)
  between operations  0.64 us (2%)
    pallas_call x1, Pallas kernels, on_device(): pl.pallas_call(functools.partial(kernel, n_sp, n_dp), out_shape=(jax.Shap...  36.5 us
    pallas_call x1, Pallas kernels, write_out(): pl.pallas_call(writer, out_shape=tuple((jax.ShapeDtypeStruct(a.shape, a.d...  2.38 us

profile of v3, /device:TPU:0, one launch (start us, length us, event | category | flops | bytes accessed | tf_op | source)
XLA Modules:
  0.0 39.5 jit_solution(10839456635492099355)
XLA Ops:
  0.6 36.5 %gla_backward.1 = (bf16[128,1024]{1,0:T(8,128)(2,1)}, bf16[128,1024]{1,0:T(8,128)(2,1)}, bf16[128,2048]{1,0:T(8,128)(2,1)}, bf16[64,128]{1,0:T(8,128)(2,1)}, f32[64,1024]{1,0:T(8,128)}) custom-call(bf16[128,1024]{1,0:T(8,128)(2,1)} %q_hbm.1, bf16[128,1024]{1,0:T(8,128)(2,1)} %k_hbm.1, bf16[128,2048]{1,0:T(8,128)(2,1)} %v_hbm.1, bf16[128,2048]{1,0:T(8,128)(2,1)} %do_hbm.1, ...), custom_call_target="tpu_custom_call" | custom-call | tf_op jit(solution)/shard_map/gla_backward/pallas_call | solution.py:358
  37.1 2.4 %write_out.1 = (bf16[128,1024]{1,0:T(8,128)(2,1)}, bf16[128,1024]{1,0:T(8,128)(2,1)}, bf16[128,2048]{1,0:T(8,128)(2,1)}, bf16[64,128]{1,0:T(8,128)(2,1)}, f32[64,1024]{1,0:T(8,128)}) custom-call(bf16[128,1024]{1,0:T(8,128)(2,1)} %get-tuple-element.15.refs_0_, bf16[128,1024]{1,0:T(8,128)(2,1)} %get-tuple-element.16.refs_1_, ...), custom_call_target="tpu_custom_call" | custom-call | tf_op jit(solution)/shard_map/write_out/pallas_call | solution.py:333
